TPU v7x, 512 devices: a whole 4x4x16 slice. The times are simulated.
512 devices in a mesh: gr: 2 (over z_hi), fs: 32 (over z_lo, y), tp: 8 (over x, core).
Axes of the slice: x: 4, y: 4, z: 16 (z_hi: 2, z_lo: 8; z = z_hi * 8 + z_lo), core: 2. Of those that a mesh axis runs over, the one named last changes fastest.
Arguments:
- prompt: bfloat16 [8192, 2048], P(('gr', 'tp'), 'fs'), may hold values from -2.5 to 2.5
- gain_pre: float32 [2048], P(('gr', 'fs')), may hold values from 0.1 to 1.9
- gate_pre: float32 [2048, 5632], P(('gr', 'fs'), 'tp'), may hold values from -6 to 6
- up_pre: float32 [2048, 5632], P(('gr', 'fs'), 'tp'), may hold values from -6 to 6
- down_pre: float32 [2048, 5632], P(('gr', 'fs'), 'tp'), may hold values from -16 to 16
- gain_post: float32 [2048], P(('gr', 'fs')), may hold values from 0.1 to 1.9
- gate_post: float32 [2048, 5632], P(('gr', 'fs'), 'tp'), may hold values from -6 to 6
- up_post: float32 [2048, 5632], P(('gr', 'fs'), 'tp'), may hold values from -6 to 6
- down_post: float32 [2048, 5632], P(('gr', 'fs'), 'tp'), may hold values from -16 to 16
Outputs:
- result: bfloat16 [8192, 2048], P(('gr', 'tp'), 'fs')
- gate_first: bfloat16 [5632, 2048], P('fs')
- up_first: bfloat16 [5632, 2048], P('fs')
- down_first: bfloat16 [5632, 2048], P('fs')
- gate_second: bfloat16 [5632, 2048], P('fs')
- up_second: bfloat16 [5632, 2048], P('fs')
- down_second: bfloat16 [5632, 2048], P('fs')
All inputs are finite; a program needn't handle non-finite values.
Results may differ from a plain program's by a relative error of at most 0.028.
Values may be sent and summed in bfloat16 or wider, within the bound.
A program may use at most 64 MiB of HBM per device.

v0:
```python
import jax
import jax.numpy as jnp
from jax import lax
from jax.sharding import PartitionSpec as P

D = 2048
FF = 5632
norm_eps = 1e-06


def half_step(tokens_t, w_gate, w_up, w_down):
    whole = lax.all_gather(tokens_t, "fs", axis=0, tiled=True)
    widened = whole.astype(jnp.float32)
    row_scale = lax.rsqrt(jnp.sum(widened * widened, axis=0, keepdims=True) / D + norm_eps) * D ** (
        -0.5
    )
    g = jnp.dot(w_gate, whole, preferred_element_type=jnp.float32) * row_scale
    u = jnp.dot(w_up, whole, preferred_element_type=jnp.float32) * row_scale
    hidden = (jax.nn.silu(g) * u).astype(jnp.bfloat16)
    partial_value = lax.dot_general(
        w_down, hidden, (((0,), (0,)), ((), ())), preferred_element_type=jnp.float32
    )
    summed = lax.psum_scatter(
        partial_value.astype(jnp.bfloat16), "fs", scatter_dimension=0, tiled=True
    )
    return (tokens_t.astype(jnp.float32) + 0.5 * FF ** (-0.5) * summed.astype(jnp.float32)).astype(
        jnp.bfloat16
    )


def relayout(matrices):
    m = jnp.stack(matrices)
    m = m.reshape(6, 8, 4, 704).transpose(1, 0, 2, 3)
    m = lax.all_to_all(m, "tp", 0, 0, tiled=True)
    m = m.reshape(8, 6, 4, 4, 176).transpose(0, 3, 1, 2, 4).reshape(32, 24, 176)
    m = lax.all_to_all(m, "fs", 0, 0, tiled=True)
    m = lax.all_gather(m.reshape(32 * 24, 176), ("gr", "tp"), axis=0, tiled=True)
    m = m.reshape(2, 8, 32, 6, 4, 176).transpose(3, 5, 0, 2, 1, 4).reshape(6, 176, 2048)
    return tuple((m[i] for i in range(6)))


def local(prompt, gain_pre, gate_pre, up_pre, down_pre, gain_post, gate_post, up_post, down_post):
    rounded = (
        (gain_pre[:, None] * gate_pre).astype(jnp.bfloat16),
        (gain_pre[:, None] * up_pre).astype(jnp.bfloat16),
        down_pre.astype(jnp.bfloat16),
        (gain_post[:, None] * gate_post).astype(jnp.bfloat16),
        (gain_post[:, None] * up_post).astype(jnp.bfloat16),
        down_post.astype(jnp.bfloat16),
    )
    served = relayout(rounded)
    middle = half_step(prompt.T, served[0], served[1], served[2])
    result = half_step(middle, served[3], served[4], served[5])
    return (result.T, *served)


def solution(mesh):
    rows = P(("gr", "fs"))
    block = P(("gr", "fs"), "tp")
    tokens = P(("gr", "tp"), "fs")
    return jax.shard_map(
        local,
        mesh=mesh,
        in_specs=(tokens, rows, block, block, block, rows, block, block, block),
        out_specs=(tokens,) + (P("fs", None),) * 6,
        check_vma=False,
    )
```

profile of v0, /device:TPU:4, one launch (start us, length us, event | category | flops | bytes accessed | tf_op | source)
XLA Modules:
  0.0 1139.2 jit_solution(12735316528702089241)
XLA Ops:
  7.2 0.7 all-gather.6.cloned.1.call-update
  7.9 1.0 multiply_convert_fusion.2
  9.0 0.9 convert_element_type.57
  10.0 1.0 multiply_convert_fusion
  11.1 0.9 convert_element_type.60
  12.2 13.6 %all_to_all.10 = bf16[8,6,4,704]{3,2,1,0:T(4,128)(2,1)S(1)} all-to-all(bf16[8,6,4,704]{3,2,1,0:T(4,128)(2,1)S(1)} %bitcast.39), channel_id=1, replica_groups=mesh['gr'=2,'fs'=32,'tp'=8] {'tp'}, dimensions={0} | all-to-all | bytes 540672 | tf_op jit(solution)/shard_map/all_to_all | solution.py:34
  25.8 0.1 copy.47
  25.9 0.3 reshape.74
  26.2 0.2 reshape.78
  26.4 0.2 copy.61
  26.6 37.4 %all_to_all.11 = bf16[32,24,176]{2,1,0:T(8,128)(2,1)} all-to-all(bf16[32,24,176]{2,1,0:T(8,128)(2,1)S(1)} %copy.61), channel_id=1, replica_groups=mesh['gr'=2,'fs'=32,'tp'=8] {'fs'}, dimensions={0} | all-to-all | bytes 540672 | tf_op jit(solution)/shard_map/all_to_all | solution.py:36
  64.1 0.0 reduce-scatter.3.cloned.1.call-start
  64.1 174.1 %all-gather.6.cloned.1.call-done = bf16[2048,512]{1,0:T(8,128)(2,1)} async-done(((bf16[64,512]{1,0:T(8,128)(2,1)}), bf16[2048,512]{1,0:T(8,128)(2,1)}) %all-gather.6.cloned.1.call-update) | async-done | bytes 2097168 | tf_op jit(solution)/shard_map/all_gather | solution.py:12
  238.2 2.1 multiply_reduce_fusion.1
  240.3 147.0 %all-gather.4.cloned.1.call-done = bf16[12288,176]{1,0:T(8,128)(2,1)} async-done(((bf16[768,176]{1,0:T(8,128)(2,1)}), bf16[12288,176]{1,0:T(8,128)(2,1)}) %all-gather.4.cloned.1.call-update) | async-done | bytes 4325392 | tf_op jit(solution)/shard_map/all_gather | solution.py:37
  387.3 9.9 reshape.77
  397.2 6.0 fusion.21
  403.2 1.6 copy.50
  404.8 2.5 squeeze.19
  407.3 2.8 copy.49
  410.1 2.5 squeeze.18
  412.6 2.8 copy.51
  415.4 2.5 squeeze.20
  417.9 2.5 convolution_multiply_fusion.3
  420.4 4.8 convolution_convert_fusion.1
  425.2 0.0 all-gather.8.cloned.1.call-start
  425.3 238.4 %reduce-scatter.3.cloned.1.call-done = bf16[64,512]{1,0:T(8,128)(2,1)} async-done(((bf16[2048,512]{1,0:T(8,128)(2,1)}), bf16[64,512]{1,0:T(8,128)(2,1)}) %reduce-scatter.3.cloned.1.call-update) | async-done | bytes 65552 | tf_op jit(solution)/shard_map/reduce_scatter | solution.py:23
  663.7 1.5 add_convert_fusion.1
  665.2 0.2 reduce-scatter.5.cloned.1.call-start
  665.5 1.6 copy.53
  667.0 1.7 squeeze.22
  668.7 1.6 copy.52
  670.3 1.7 squeeze.21
  672.0 1.6 copy.54
  673.6 1.7 squeeze.23
  675.3 205.9 %all-gather.8.cloned.1.call-done = bf16[2048,512]{1,0:T(8,128)(2,1)} async-done(((bf16[64,512]{1,0:T(8,128)(2,1)}), bf16[2048,512]{1,0:T(8,128)(2,1)}) %all-gather.8.cloned.1.call-update) | async-done | bytes 2097168 | tf_op jit(solution)/shard_map/all_gather | solution.py:12
  881.3 2.2 multiply_reduce_fusion
  883.5 0.6 convolution_multiply_fusion.1
  884.1 4.2 convolution_convert_fusion
  888.3 1.2 copy-done
  889.5 1.2 copy.55
  890.7 1.2 copy.56
  892.0 1.2 copy.57
  893.2 1.2 copy.58
  894.4 1.2 copy.59
  895.6 1.2 copy.60
  896.8 234.4 %reduce-scatter.5.cloned.1.call-done = bf16[64,512]{1,0:T(8,128)(2,1)} async-done(((bf16[2048,512]{1,0:T(8,128)(2,1)}), bf16[64,512]{1,0:T(8,128)(2,1)}) %reduce-scatter.5.cloned.1.call-update) | async-done | bytes 65552 | tf_op jit(solution)/shard_map/reduce_scatter | solution.py:23
  1131.1 1.5 fusion.18
  (43 shorter events, 0.5 us)
Async XLA Ops:
  7.2 231.0 %all-gather.6.cloned.1.call-start = ((), (), s32[]{:S(2)}) async-start(), calls=%async_computation.5 | async-start | bytes 2162688 | tf_op jit(solution)/shard_map/all_gather | solution.py:12
  7.9 379.4 %all-gather.4.cloned.1.call-start = ((), (), s32[]{:S(2)}) async-start(), calls=%async_computation.4 | async-start | bytes 6684672 | tf_op jit(solution)/shard_map/all_gather | solution.py:37
  64.1 599.7 %reduce-scatter.3.cloned.1.call-start = ((), (), s32[]{:S(2)}) async-start(), calls=%async_computation.6 | async-start | bytes 2162688 | tf_op jit(solution)/shard_map/reduce_scatter | solution.py:23
  425.2 238.5 %copy-start.11 = (bf16[512,64]{0,1:T(8,128)(2,1)S(1)}, bf16[512,64]{0,1:T(8,128)(2,1)}, u32[]{:S(2)}) copy-start(bf16[512,64]{0,1:T(8,128)(2,1)} %param.9) | copy-start | bytes 196612
  425.2 456.0 %all-gather.8.cloned.1.call-start = ((), (), s32[]{:S(2)}) async-start(), calls=%async_computation.7 | async-start | bytes 2162688 | tf_op jit(solution)/shard_map/all_gather | solution.py:12
  665.2 465.9 %reduce-scatter.5.cloned.1.call-start = ((), (), s32[]{:S(2)}) async-start(), calls=%async_computation.8 | async-start | bytes 2162688 | tf_op jit(solution)/shard_map/reduce_scatter | solution.py:23
  668.7 214.8 %copy-start.3 = (bf16[176,2048]{0,1:T(8,128)(2,1)}, bf16[176,2048]{0,1:T(8,128)(2,1)S(1)}, u32[]{:S(2)}) copy-start(bf16[176,2048]{0,1:T(8,128)(2,1)S(1)} %squeeze.22) | copy-start | bytes 2162692
  672.0 212.1 %copy-start.5 = (bf16[176,2048]{0,1:T(8,128)(2,1)}, bf16[176,2048]{0,1:T(8,128)(2,1)S(1)}, u32[]{:S(2)}) copy-start(bf16[176,2048]{0,1:T(8,128)(2,1)S(1)} %squeeze.21) | copy-start | bytes 2162692
  675.3 208.8 %copy-start.7 = (bf16[176,2048]{0,1:T(8,128)(2,1)}, bf16[176,2048]{0,1:T(8,128)(2,1)S(1)}, u32[]{:S(2)}) copy-start(bf16[176,2048]{0,1:T(8,128)(2,1)S(1)} %squeeze.23) | copy-start | bytes 2162692
  881.3 2.3 copy-start.9
  888.3 1.2 copy-start
  888.3 2.4 copy-start.2
  889.5 2.4 copy-start.1
  890.7 2.4 copy-start.4
  891.9 2.4 copy-start.8
  893.2 2.4 copy-start.6
  894.4 236.8 %copy-start.10 = (bf16[64,512]{1,0:T(8,128)(2,1)S(1)}, bf16[64,512]{1,0:T(8,128)(2,1)}, u32[]{:S(2)}) copy-start(bf16[64,512]{1,0:T(8,128)(2,1)} %add_convert_fusion.1) | copy-start | bytes 196612
Sparse Core Ops, SparseCore 0:
  10.1 228.0 all-gather.5
  241.5 145.7 all-gather.3
  425.4 238.3 reduce-scatter.2
  666.2 214.9 all-gather.7
  888.4 242.6 reduce-scatter.4
where the time goes:
time: 1140 us
  waiting for transfers between devices  1000 us (88%)
  blocking collectives  51 us (4%)
  local copies, waits for them, and re-layouts  50 us (4%)
  between operations  14 us (1%)
  matrix products  12.1 us (1%)
    reduce_scatter x2, waiting for transfers between devices, half_step(): lax.psum_scatter(partial_value.astype(jnp.bfloat16), 'fs', scatter_dimens...  473 us
    all_gather x2, waiting for transfers between devices, half_step(): whole = lax.all_gather(tokens_t, 'fs', axis=0, tiled=True)  380 us
    all_gather x1, waiting for transfers between devices, relayout(): lax.all_gather(m.reshape(32 * 24, 176), ('gr', 'tp'), axis=0, tiled=True)  147 us
    all_to_all x1, blocking collectives, relayout(): m = lax.all_to_all(m, 'fs', 0, 0, tiled=True)  37.4 us
  transfers between devices with their start and end apart: 5, of which 5 were waited for; matrix products, arithmetic and copies ran while one was open for 2% of the time, Pallas kernels for 0%

commit v1 on v0

--- a/solution.py
+++ b/solution.py
@@ -9,7 +9,10 @@
 
 
 def half_step(tokens_t, w_gate, w_up, w_down):
-    whole = lax.all_gather(tokens_t, "fs", axis=0, tiled=True)
+    size = lax.axis_size("fs")
+    blocks = jnp.stack([tokens_t for _ in range(size)])
+    blocks = lax.all_to_all(blocks, "fs", split_axis=0, concat_axis=0)
+    whole = jnp.concatenate(blocks, axis=0)
     widened = whole.astype(jnp.float32)
     row_scale = lax.rsqrt(jnp.sum(widened * widened, axis=0, keepdims=True) / D + norm_eps) * D ** (
         -0.5

time: 1140 us -> 876 us (0.77)
  the two profiles are of different devices: /device:TPU:4 before, /device:TPU:6 now
where the time goes in v1:
time: 876 us; the launch traced here: 875 us
  waiting for transfers between devices  723 us (83%)
  local copies, waits for them, and re-layouts  58.3 us (7%)
  blocking collectives  50.3 us (6%)
  between operations  13.9 us (2%)
  matrix products  12.2 us (1%)
  starting transfers between devices  10.2 us (1%)
    reduce_scatter x2, waiting for transfers between devices, half_step(): lax.psum_scatter(partial_value.astype(jnp.bfloat16), 'fs', scatter_dimens...  495 us
    all_to_all x2, waiting for transfers between devices, half_step(): blocks = lax.all_to_all(blocks, 'fs', split_axis=0, concat_axis=0)  224 us
    all_to_all x1, blocking collectives, relayout(): m = lax.all_to_all(m, 'fs', 0, 0, tiled=True)  36.2 us
    slice x7, local copies, waits for them, and re-layouts, relayout(): return tuple((m[i] for i in range(6)))  20.6 us
  transfers between devices with their start and end apart: 5, of which 5 were waited for; matrix products, arithmetic and copies ran while one was open for 3% of the time, Pallas kernels for 0%

profile of v1, /device:TPU:6, one launch (start us, length us, event | category | flops | bytes accessed | tf_op | source)
XLA Modules:
  0.0 875.1 jit_solution(16320196857466334367)
XLA Ops:
  7.2 1.0 multiply_convert_fusion.2
  8.3 0.9 convert_element_type.59
  9.2 1.0 multiply_convert_fusion
  10.3 0.9 convert_element_type.62
  11.4 14.1 %all_to_all.20 = bf16[8,6,4,704]{3,2,1,0:T(4,128)(2,1)S(1)} all-to-all(bf16[8,6,4,704]{3,2,1,0:T(4,128)(2,1)S(1)} %bitcast.45), channel_id=1, replica_groups=mesh['gr'=2,'fs'=32,'tp'=8] {'tp'}, dimensions={0} | all-to-all | bytes 540672 | tf_op jit(solution)/shard_map/all_to_all | solution.py:37
  25.6 0.3 reshape.84
  25.9 0.2 reshape.90
  26.1 0.2 copy.75
  26.4 36.2 %all_to_all.21 = bf16[32,24,176]{2,1,0:T(8,128)(2,1)} all-to-all(bf16[32,24,176]{2,1,0:T(8,128)(2,1)S(1)} %copy.75), channel_id=1, replica_groups=mesh['gr'=2,'fs'=32,'tp'=8] {'fs'}, dimensions={0} | all-to-all | bytes 540672 | tf_op jit(solution)/shard_map/all_to_all | solution.py:39
  62.6 1.6 stack.25
  64.1 5.8 all-to-all-start.2
  70.0 0.7 all-gather.2.cloned.1.call-update
  70.8 167.8 %all-to-all-done.2 = bf16[32,64,512]{2,1,0:T(8,128)(2,1)S(1)} async-done(((bf16[32,64,512]{2,1,0:T(8,128)(2,1)}), bf16[32,64,512]{2,1,0:T(8,128)(2,1)S(1)}, u32[]{:S(2)}, u32[]{:S(2)}) %all-to-all-start.2) | async-done | bytes 2097184 | tf_op jit(solution)/shard_map/all_to_all | solution.py:14
  238.6 0.6 multiply_reduce_fusion.1
  239.1 3.7 all-gather.2.cloned.1.call-done
  242.8 9.9 %reshape.87 = bf16[2,8,32,6,4,176]{5,4,3,2,1,0:T(4,128)(2,1)} reshape(bf16[12288,176]{1,0:T(8,128)(2,1)} %all-gather.2.cloned.1.call-done) | data formatting | bytes 8650752 | tf_op jit(solution)/shard_map/reshape | solution.py:41
  252.7 6.2 fusion.21
  258.9 1.6 copy.64
  260.5 2.5 squeeze.19
  263.0 2.8 copy.63
  265.8 2.5 squeeze.18
  268.2 2.8 copy.65
  271.0 2.5 squeeze.20
  273.5 2.5 convolution_multiply_fusion.3
  276.0 4.2 convolution_convert_fusion.1
  280.3 259.3 %reduce-scatter.3.cloned.1.call-done = bf16[64,512]{1,0:T(8,128)(2,1)} async-done(((bf16[2048,512]{1,0:T(8,128)(2,1)}), bf16[64,512]{1,0:T(8,128)(2,1)}) %reduce-scatter.3.cloned.1.call-update) | async-done | bytes 65552 | tf_op jit(solution)/shard_map/reduce_scatter | solution.py:26
  539.6 0.9 add_convert_fusion.1
  540.5 1.6 stack.26
  542.0 4.0 all-to-all-start.3
  546.3 2.9 copy.67
  549.1 2.5 squeeze.22
  551.6 2.8 copy.66
  554.5 2.5 squeeze.21
  556.9 1.6 copy.68
  558.6 2.6 squeeze.23
  561.2 55.8 %all-to-all-done.3 = bf16[32,64,512]{2,1,0:T(8,128)(2,1)S(1)} async-done(((bf16[32,64,512]{2,1,0:T(8,128)(2,1)}), bf16[32,64,512]{2,1,0:T(8,128)(2,1)S(1)}, u32[]{:S(2)}, u32[]{:S(2)}) %all-to-all-start.3) | async-done | bytes 2097184 | tf_op jit(solution)/shard_map/all_to_all | solution.py:14
  617.0 0.6 multiply_reduce_fusion
  617.6 1.3 convolution_multiply_fusion.1
  618.9 4.2 convolution_convert_fusion
  623.1 1.2 copy-done
  624.3 1.2 copy.69
  625.5 1.2 copy.70
  626.7 1.2 copy.71
  627.9 1.2 copy.72
  629.2 1.2 copy.73
  630.4 1.2 copy.74
  631.6 235.5 %reduce-scatter.5.cloned.1.call-done = bf16[64,512]{1,0:T(8,128)(2,1)} async-done(((bf16[2048,512]{1,0:T(8,128)(2,1)}), bf16[64,512]{1,0:T(8,128)(2,1)}) %reduce-scatter.5.cloned.1.call-update) | async-done | bytes 65552 | tf_op jit(solution)/shard_map/reduce_scatter | solution.py:26
  867.0 1.5 fusion.18
  (35 shorter events, 0.7 us)
Async XLA Ops:
  11.4 51.2 %copy-start.7 = (bf16[512,64]{0,1:T(8,128)(2,1)S(1)}, bf16[512,64]{0,1:T(8,128)(2,1)}, u32[]{:S(2)}) copy-start(bf16[512,64]{0,1:T(8,128)(2,1)} %param.9) | copy-start | bytes 196612
  64.1 174.4 %all-to-all-start.2 = ((bf16[32,64,512]{2,1,0:T(8,128)(2,1)}), bf16[32,64,512]{2,1,0:T(8,128)(2,1)S(1)}, u32[]{:S(2)}, u32[]{:S(2)}) async-start(bf16[32,64,512]{2,1,0:T(8,128)(2,1)} %stack.25), calls=%async_computation.2 | async-start | bytes 4194304 | tf_op jit(solution)/shard_map/all_to_all | solution.py:14
  70.0 172.8 %all-gather.2.cloned.1.call-start = ((), (), s32[]{:S(2)}) async-start(), calls=%async_computation.6 | async-start | bytes 6684672 | tf_op jit(solution)/shard_map/all_gather | solution.py:40
  70.7 468.9 %reduce-scatter.3.cloned.1.call-start = ((), (), s32[]{:S(2)}) async-start(), calls=%async_computation.7 | async-start | bytes 2162688 | tf_op jit(solution)/shard_map/reduce_scatter | solution.py:26
  542.0 75.0 %all-to-all-start.3 = ((bf16[32,64,512]{2,1,0:T(8,128)(2,1)}), bf16[32,64,512]{2,1,0:T(8,128)(2,1)S(1)}, u32[]{:S(2)}, u32[]{:S(2)}) async-start(bf16[32,64,512]{2,1,0:T(8,128)(2,1)} %stack.26), calls=%async_computation.4 | async-start | bytes 4194304 | tf_op jit(solution)/shard_map/all_to_all | solution.py:14
  546.1 321.0 %reduce-scatter.5.cloned.1.call-start = ((), (), s32[]{:S(2)}) async-start(), calls=%async_computation.8 | async-start | bytes 2162688 | tf_op jit(solution)/shard_map/reduce_scatter | solution.py:26
  558.6 59.0 %copy-start.3 = (bf16[176,2048]{0,1:T(8,128)(2,1)S(1)}, bf16[176,2048]{0,1:T(8,128)(2,1)}, u32[]{:S(2)}) copy-start(bf16[176,2048]{0,1:T(8,128)(2,1)} %squeeze.22) | copy-start | bytes 2162692
  623.1 1.2 copy-start
  623.1 2.4 copy-start.2
  624.3 2.4 copy-start.1
  625.5 2.4 copy-start.4
  626.7 2.4 copy-start.6
  627.9 2.4 copy-start.5
Sparse Core Ops, SparseCore 0:
  74.1 168.6 all-gather.1
  280.4 259.1 reduce-scatter.2
  623.2 243.7 reduce-scatter.4
